TPU v7x, 32 devices: a whole 2x2x4 slice. The times are simulated.
32 devices in a mesh: kv: 8 (over z, y), tp: 4 (over x, core).
Axes of the slice: x: 2, y: 2, z: 4, core: 2. Of those that a mesh axis runs over, the one named last changes fastest.
Arguments:
- tokens: bfloat16 [16, 4096], P(None, 'tp'), may hold values from -6 to 6
- norm_gain: float32 [4096], P('tp'), may hold values from 0.1 to 1.9
- w_query: bfloat16 [4096, 32, 96], P('tp', 'kv'), as said below
- w_latent: bfloat16 [4096, 1024], P('tp', 'kv'), may hold values from -0.09375 to 0.09375
- w_rotary: bfloat16 [4096, 32], P('tp'), may hold values from -0.09375 to 0.09375
- latent_gain: float32 [1024], replicated, may hold values from 0.1 to 1.9
- w_key_up: bfloat16 [1024, 32, 64], P('tp', 'kv'), may hold values from -0.1875 to 0.1875
- w_value_up: bfloat16 [1024, 32, 128], replicated, may hold values from -0.1875 to 0.1875
- w_out: bfloat16 [4096, 4096], P('kv', 'tp'), may hold values from -0.09375 to 0.09375
- cache_latent: bfloat16 [16, 4096, 1024], P(None, ('kv', 'tp')), may hold values from -6 to 6
- cache_rotary: bfloat16 [16, 4096, 32], P(None, ('kv', 'tp')), may hold values from -6 to 6
- lengths: int32 [16], replicated, may hold values from 1024 to 4096
Outputs:
- mixed_out: bfloat16 [16, 4096], P(None, 'tp')
- new_latent: bfloat16 [16, 1024], P(None, ('kv', 'tp'))
- new_rotary: bfloat16 [16, 32], replicated
Inputs may be any that keep to these rules, and one draw needn't show every extreme that they name: `w_query`: finite.
All inputs are finite; a program needn't handle non-finite values.
Results may differ from a plain program's by a relative error of at most 0.012.
The roundings to bfloat16 on the way count: a program that leaves them out, or rounds other values in their place, can miss the bound.
Values may be sent and summed in bfloat16 or wider, within the bound.
A program may use at most 64 MiB of HBM per device.

v0:
```python
import jax
import jax.numpy as jnp
from jax import lax
from jax.sharding import PartitionSpec as P

THETA = 10000.0
EPS = 1e-06


def rotate(values, position):
    full_width = values.shape[-1]
    half_width = full_width // 2
    frequency = THETA ** (-jnp.arange(0, full_width, 2, dtype=jnp.float32) / full_width)
    angles = position.astype(jnp.float32)[:, None] * frequency[None, :]
    angles = angles.reshape((angles.shape[0],) + (1,) * (values.ndim - 2) + (half_width,))
    cosine = jnp.cos(angles)
    sine_part = jnp.sin(angles)
    first_half = values[..., :half_width]
    second_half = values[..., half_width:]
    return jnp.concatenate(
        [
            first_half * cosine - second_half * sine_part,
            first_half * sine_part + second_half * cosine,
        ],
        axis=-1,
    )


def value_product(latent_f, weight):
    high_part = latent_f.astype(jnp.bfloat16)
    low_part = (latent_f - high_part.astype(jnp.float32)).astype(jnp.bfloat16)
    return jnp.einsum(
        "bhr,rhv->bhv", high_part, weight, preferred_element_type=jnp.float32
    ) + jnp.einsum("bhr,rhv->bhv", low_part, weight, preferred_element_type=jnp.float32)


def shards(
    tokens,
    norm_gain,
    w_query,
    w_latent,
    w_rotary,
    latent_gain,
    w_key_up,
    w_value_up,
    w_out,
    cache_latent,
    cache_rotary,
    lengths,
):
    seq_count = tokens.shape[0]
    kv_count = lax.axis_size("kv")
    tp_count = lax.axis_size("tp")
    kv_index = lax.axis_index("kv")
    tp_index = lax.axis_index("tp")
    heads_dev = w_query.shape[1]
    head_count = heads_dev * kv_count
    latent_rank = cache_latent.shape[2]
    rope_width = cache_rotary.shape[2]
    nope_width = w_query.shape[2] - rope_width
    model_width = tokens.shape[1] * tp_count
    score_scale = w_query.shape[2] ** (-0.5)
    tokens_f = tokens.astype(jnp.float32)
    scaled = (tokens_f * norm_gain).astype(jnp.bfloat16)
    query_part = jnp.einsum("bd,dhn->bhn", scaled, w_query, preferred_element_type=jnp.float32)
    latent_part = jnp.dot(scaled, w_latent, preferred_element_type=jnp.float32)
    rotary_part = jnp.dot(scaled, w_rotary, preferred_element_type=jnp.float32)
    square_part = jnp.sum(tokens_f * tokens_f, axis=1)
    query_sum, latent_sum, rotary_sum, square_sum = lax.psum(
        (query_part, latent_part, rotary_part, square_part), "tp"
    )
    inverse = lax.rsqrt(square_sum / model_width + EPS)
    query_heads = (query_sum * inverse[:, None, None]).astype(jnp.bfloat16)
    compressed = (latent_sum * inverse[:, None]).astype(jnp.bfloat16)
    new_rotary = rotate(rotary_sum * inverse[:, None], lengths).astype(jnp.bfloat16)
    query_rope = rotate(query_heads[:, :, nope_width:].astype(jnp.float32), lengths).astype(
        jnp.bfloat16
    )
    query_latent = jnp.einsum(
        "bhn,rhn->bhr", query_heads[:, :, :nope_width], w_key_up, preferred_element_type=jnp.float32
    ).astype(jnp.bfloat16)
    rope_slice = rope_width // tp_count
    column_slice = compressed.shape[1] // tp_count
    rope_piece = lax.dynamic_slice_in_dim(query_rope, tp_index * rope_slice, rope_slice, 2)
    column_piece = lax.dynamic_slice_in_dim(compressed, tp_index * column_slice, column_slice, 1)
    got_latent, got_rope, got_columns = (
        lax.all_gather(query_latent[:, None], ("kv", "tp"), axis=1, tiled=True),
        lax.all_gather(rope_piece[:, None], ("kv", "tp"), axis=1, tiled=True),
        lax.all_gather(column_piece[:, None], ("kv", "tp"), axis=1, tiled=True),
    )
    rank_slice = query_latent.shape[2]
    all_latent = got_latent.reshape(seq_count, kv_count, tp_count, heads_dev, rank_slice)
    all_latent = all_latent.transpose(0, 1, 3, 2, 4).reshape(seq_count, head_count, latent_rank)
    all_rope = got_rope.reshape(seq_count, kv_count, tp_count, heads_dev, rope_slice)
    all_rope = all_rope.transpose(0, 1, 3, 2, 4).reshape(seq_count, head_count, rope_width)
    fresh_f = got_columns.reshape(seq_count, latent_rank).astype(jnp.float32)
    new_latent = (
        fresh_f * lax.rsqrt(jnp.mean(fresh_f * fresh_f, axis=1, keepdims=True) + EPS) * latent_gain
    ).astype(jnp.bfloat16)
    new_latent_f = new_latent.astype(jnp.float32)
    own_score = (
        jnp.einsum("bhr,br->bh", all_latent, new_latent, preferred_element_type=jnp.float32)
        + jnp.einsum("bhq,bq->bh", all_rope, new_rotary, preferred_element_type=jnp.float32)
    ) * score_scale
    pos_dev = cache_latent.shape[1]
    first_pos = (kv_index * tp_count + tp_index) * pos_dev
    position = first_pos + jnp.arange(pos_dev, dtype=jnp.int32)
    valid = position[None, :] < lengths[:, None]
    scores = (
        jnp.einsum("bhr,bpr->bhp", all_latent, cache_latent, preferred_element_type=jnp.float32)
        + jnp.einsum("bhq,bpq->bhp", all_rope, cache_rotary, preferred_element_type=jnp.float32)
    ) * score_scale
    masked = jnp.where(valid[:, None, :], scores, -jnp.inf)
    local_top = jnp.maximum(jnp.max(masked, axis=2), own_score)
    top_score = lax.pmax(local_top, ("kv", "tp"))
    weights = jnp.where(valid[:, None, :], jnp.exp(scores - top_score[:, :, None]), 0.0)
    total_part = jnp.sum(weights, axis=2)
    summed_part = jnp.einsum(
        "bhp,bpr->bhr",
        weights.astype(jnp.bfloat16),
        cache_latent,
        preferred_element_type=jnp.float32,
    )
    own_weight = jnp.exp(own_score - top_score)
    block_own = lax.dynamic_slice_in_dim(own_weight, kv_index * heads_dev, heads_dev, 1)
    value_block_weight = lax.dynamic_slice_in_dim(w_value_up, kv_index * heads_dev, heads_dev, 1)
    totals, summed = lax.psum((total_part, summed_part), ("kv", "tp"))
    block_sum = lax.dynamic_slice_in_dim(summed, kv_index * heads_dev, heads_dev, 1)
    block_total = lax.dynamic_slice_in_dim(totals, kv_index * heads_dev, heads_dev, 1)
    latent_out = (block_sum + block_own[:, :, None] * new_latent_f[:, None, :]) / (
        block_total + block_own
    )[:, :, None]
    head_out = value_product(latent_out, value_block_weight).astype(jnp.bfloat16)
    out_part = jnp.dot(head_out.reshape(seq_count, -1), w_out, preferred_element_type=jnp.float32)
    mixed_out = lax.psum(out_part, "kv").astype(jnp.bfloat16)
    latent_width = latent_rank // (kv_count * tp_count)
    latent_piece = lax.dynamic_slice_in_dim(
        new_latent, (kv_index * tp_count + tp_index) * latent_width, latent_width, 1
    )
    return (mixed_out, latent_piece, new_rotary)


def solution(mesh):
    placed = (
        P(None, "tp"),
        P("tp"),
        P("tp", "kv", None),
        P("tp", "kv"),
        P("tp", None),
        P(),
        P("tp", "kv", None),
        P(),
        P("kv", "tp"),
        P(None, ("kv", "tp"), None),
        P(None, ("kv", "tp"), None),
        P(),
    )
    return jax.shard_map(
        shards,
        mesh=mesh,
        in_specs=placed,
        out_specs=(P(None, "tp"), P(None, ("kv", "tp")), P()),
        check_vma=False,
    )
```

profile of v0, /device:TPU:0, one launch (start us, length us, event | category | flops | bytes accessed | tf_op | source)
XLA Modules:
  0.0 341.0 jit_solution(9099277364081239508)
XLA Ops:
  7.2 0.0 all-gather.6.cloned.1.call-start
  7.2 1.0 fusion.15
  8.2 1.5 fusion.20
  9.7 1.0 fusion.22
  10.7 1.1 fusion.24
  11.9 13.4 %all-reduce = (f32[16,4,96]{2,0,1:T(8,128)S(1)}, f32[16]{0:T(128)S(1)}, f32[16,128]{1,0:T(8,128)S(1)}, f32[16,32]{1,0:T(8,128)S(1)}) all-reduce(f32[16,4,96]{2,0,1:T(8,128)S(1)} %fusion.20, f32[16]{0:T(128)S(1)} %fusion.15, f32[16,128]{1,0:T(8,128)S(1)} %fusion.24, f32[16,32]{1,0:T(8,128)S(1)} %fusion.22), channel_id=1, replica_groups=mesh['kv'=8,'tp'=4] {'tp'}, use_global_device_ids=true, to_apply=%region_0.0 | all-reduce | flops 8720 | bytes 69760 | tf_op jit(solution)/shard_map/psum | solution.py:69
  25.3 0.1 multiply_convert_fusion.1
  25.3 1.7 fusion.1
  27.0 0.0 all-gather.6.cloned.1.call-update
  27.0 0.0 all-reduce.3.cloned.1.call-start
  27.1 0.7 convert_element_type.81
  27.8 0.1 broadcast_multiply_fusion
  27.8 0.1 subtract_convert_fusion.3
  28.0 0.1 slice_convert_fusion
  28.0 0.1 subtract_convert_fusion.2
  28.1 0.1 dynamic-slice_maximum_fusion
  28.2 0.1 copy.48
  28.3 41.5 %all-gather.1 = bf16[16,128,8]{0,2,1:T(8,128)(2,1)S(1)} all-gather(bf16[16,4,8]{0,2,1:T(8,128)(2,1)S(1)} %copy.48), channel_id=3, replica_groups=mesh['kv'=8,'tp'=4] {'kv','tp'}, dimensions={1}, use_global_device_ids=true | all-gather | bytes 33792 | tf_op jit(solution)/shard_map/all_gather | solution.py:88
  69.8 0.3 copy.50
  70.1 37.0 %all-gather.3 = bf16[32,32,16]{1,2,0:T(8,128)(2,1)S(1)} all-gather(bf16[1,32,16]{1,2,0:T(8,128)(2,1)S(1)} %get-tuple-element.20), channel_id=4, replica_groups=mesh['kv'=8,'tp'=4] {'kv','tp'}, dimensions={0}, use_global_device_ids=true | all-gather | bytes 33792 | tf_op jit(solution)/shard_map/all_gather | solution.py:89
  107.1 0.1 reshape.167
  107.3 0.1 fusion.54
  107.3 0.1 multiply_reduce_fusion
  107.5 0.7 broadcast_compare_fusion
  108.2 0.2 fusion.33
  108.4 0.1 bitcast_convert_fusion
  108.5 0.0 all-gather.6.cloned.1.call-done
  108.5 2.0 copy.75
  110.6 0.8 reshape.151
  111.3 3.7 %fusion.41 = f32[16,32,128]{2,1,0:T(8,128)S(1)} fusion(bf16[16,32,1024]{2,1,0:T(8,128)(2,1)S(1)} %reshape.151, bf16[16,128,1024]{2,1,0:T(8,128)(2,1)} %param.21), kind=kOutput, calls=%fused_computation.71 | convolution fusion | flops 134217728 | bytes 5505024 | tf_op jit(solution)/shard_map/bhr,bpr->bhp/dot_general | solution.py:110
  115.0 0.4 fusion.16
  115.4 0.3 select_reduce_fusion
  115.7 37.0 %pmax.7 = f32[16,32]{1,0:T(8,128)S(1)} all-reduce(f32[16,32]{1,0:T(8,128)S(1)} %get-tuple-element.11), channel_id=1, replica_groups=mesh['kv'=8,'tp'=4] {'kv','tp'}, use_global_device_ids=true, to_apply=%region_7.8 | all-reduce | flops 512 | bytes 4096 | tf_op jit(solution)/shard_map/pmax | solution.py:115
  152.7 2.9 fusion.9
  155.6 2.5 copy.52
  158.2 0.7 pad_maximum_fusion
  158.9 0.7 dynamic-slice_bitcast_fusion
  159.5 2.1 constant_dynamic-slice_fusion
  161.7 0.3 fusion.7
  161.9 42.7 %psum.54 = f32[16,32]{1,0:T(8,128)S(1)} all-reduce(f32[16,32]{1,0:T(8,128)S(1)} %fusion.7), channel_id=1, replica_groups=mesh['kv'=8,'tp'=4] {'kv','tp'}, use_global_device_ids=true, to_apply=%region_10.11 | all-reduce | flops 512 | bytes 4096 | tf_op jit(solution)/shard_map/psum | solution.py:127
  204.6 0.1 dynamic-slice_add_fusion
  204.7 0.1 copy.53
  204.8 0.1 copy.54
  204.8 89.8 %all-reduce.3.cloned.1.call-done = f32[16,32,1024]{2,0,1:T(8,128)} async-done(((f32[16,32,1024]{2,0,1:T(8,128)}), f32[16,32,1024]{2,0,1:T(8,128)}) %all-reduce.3.cloned.1.call-update) | async-done | bytes 2097168 | tf_op jit(solution)/shard_map/psum | solution.py:127
  294.6 1.3 fusion.4
  295.9 1.3 fusion.3
  297.2 0.3 fusion.27
  297.4 36.8 %psum.55 = bf16[16,1024]{1,0:T(8,128)(2,1)} all-reduce(f32[16,1024]{1,0:T(8,128)S(1)} %fusion.27), channel_id=1, replica_groups=mesh['kv'=8,'tp'=4] {'kv'}, use_global_device_ids=true, to_apply=%region_11.12 | all-reduce | flops 16384 | bytes 98304 | tf_op jit(solution)/shard_map/psum | solution.py:135
  (14 shorter events, 0.1 us)
Async XLA Ops:
  7.2 290.0 %copy-start = (bf16[512,1024]{1,0:T(8,128)(2,1)S(1)}, bf16[512,1024]{1,0:T(8,128)(2,1)}, u32[]{:S(2)}) copy-start(bf16[512,1024]{1,0:T(8,128)(2,1)} %param.20) | copy-start | bytes 3145732
  7.2 101.2 %copy-start.2 = (f32[1024]{0:T(1024)S(1)}, f32[1024]{0:T(1024)}, u32[]{:S(2)}) copy-start(f32[1024]{0:T(1024)} %param.17) | copy-start | bytes 12292
  7.2 101.3 %all-gather.6.cloned.1.call-start = ((), (), s32[]{:S(2)}) async-start(), calls=%async_computation.1 | async-start | bytes 1081344 | tf_op jit(solution)/shard_map/all_gather | solution.py:87
  27.0 267.6 %all-reduce.3.cloned.1.call-start = ((), (), s32[]{:S(2)}) async-start(), calls=%async_computation | async-start | bytes 4194304 | tf_op jit(solution)/shard_map/psum | solution.py:127
  110.5 4.9 %copy-start.1 = (bf16[16,128,32]{1,2,0:T(8,128)(2,1)S(1)}, bf16[16,128,32]{1,2,0:T(8,128)(2,1)}, u32[]{:S(2)}) copy-start(bf16[16,128,32]{1,2,0:T(8,128)(2,1)} %param.22) | copy-start | bytes 393220
Sparse Core Ops, SparseCore 0:
  27.1 54.0 all-gather.5
  158.3 136.2 all-reduce.2
where the time goes:
time: 342 us; the launch traced here: 341 us
  blocking collectives  208 us (61%)
  waiting for transfers between devices  89.9 us (26%)
  matrix products  15.6 us (5%)
  between operations  14.2 us (4%)
  local copies, waits for them, and re-layouts  8.86 us (3%)
  other arithmetic  4.22 us (1%)
    psum x1, waiting for transfers between devices, shards(): totals, summed = lax.psum((total_part, summed_part), ('kv', 'tp'))  89.8 us
    psum x1, blocking collectives, shards(): totals, summed = lax.psum((total_part, summed_part), ('kv', 'tp'))  42.7 us
    all_gather x1, blocking collectives, shards(): lax.all_gather(rope_piece[:, None], ('kv', 'tp'), axis=1, tiled=True)  41.5 us
    all_gather x1, blocking collectives, shards(): lax.all_gather(column_piece[:, None], ('kv', 'tp'), axis=1, tiled=True)  37 us
    pmax x1, blocking collectives, shards(): top_score = lax.pmax(local_top, ('kv', 'tp'))  37 us
    psum x1, blocking collectives, shards(): mixed_out = lax.psum(out_part, 'kv').astype(jnp.bfloat16)  36.8 us
    psum x1, blocking collectives, shards(): lax.psum((query_part, latent_part, rotary_part, square_part), 'tp')  13.4 us
  transfers between devices with their start and end apart: 2, of which 1 were waited for; matrix products, arithmetic and copies ran while one was open for 2% of the time, Pallas kernels for 0%

commit v1 on v0

--- a/solution.py
+++ b/solution.py
@@ -1,3 +1,4 @@
+import functools
 import jax
 import jax.numpy as jnp
 from jax import lax
@@ -5,6 +6,15 @@
 
 THETA = 10000.0
 EPS = 1e-06
+
+
+def supply_the_scenes(array_here, link_axis, row_axis):
+    for at in (link_axis, row_axis):
+        array_here = lax.psum(array_here, at)
+    return array_here
+
+
+begin_the_types = functools.partial(supply_the_scenes, link_axis="kv", row_axis="tp")
 
 
 def rotate(values, position):
@@ -124,7 +134,7 @@
     own_weight = jnp.exp(own_score - top_score)
     block_own = lax.dynamic_slice_in_dim(own_weight, kv_index * heads_dev, heads_dev, 1)
     value_block_weight = lax.dynamic_slice_in_dim(w_value_up, kv_index * heads_dev, heads_dev, 1)
-    totals, summed = lax.psum((total_part, summed_part), ("kv", "tp"))
+    totals, summed = begin_the_types((total_part, summed_part))
     block_sum = lax.dynamic_slice_in_dim(summed, kv_index * heads_dev, heads_dev, 1)
     block_total = lax.dynamic_slice_in_dim(totals, kv_index * heads_dev, heads_dev, 1)
     latent_out = (block_sum + block_own[:, :, None] * new_latent_f[:, None, :]) / (

time: 342 us -> 364 us (1.064)
  waiting for transfers between devices: 89.9 us -> 128 us
  blocking collectives: 208 us -> 193 us
    psum x1 -> x2, waiting for transfers between devices: 89.8 us -> 128 us  [supply_the_scenes(): array_here = lax.psum(array_here, at)]
    psum x1 -> x2, blocking collectives: 42.7 us -> 25.6 us  [supply_the_scenes(): array_here = lax.psum(array_here, at)]
  transfers between devices with their start and end apart: 2 -> 3, of which waited for: 1 -> 2; matrix products, arithmetic and copies ran while one was open for 2% -> 2% of each run, Pallas kernels for 0% -> 0%
where the time goes in v1:
time: 364 us; the launch traced here: 363 us
  blocking collectives  193 us (53%)
  waiting for transfers between devices  128 us (35%)
  matrix products  15.6 us (4%)
  between operations  13.9 us (4%)
  local copies, waits for them, and re-layouts  8.86 us (2%)
  other arithmetic  4.23 us (1%)
    psum x2, waiting for transfers between devices, supply_the_scenes(): array_here = lax.psum(array_here, at)  128 us
    all_gather x1, blocking collectives, shards(): lax.all_gather(rope_piece[:, None], ('kv', 'tp'), axis=1, tiled=True)  41.5 us
    psum x1, blocking collectives, shards(): mixed_out = lax.psum(out_part, 'kv').astype(jnp.bfloat16)  38.1 us
    all_gather x1, blocking collectives, shards(): lax.all_gather(column_piece[:, None], ('kv', 'tp'), axis=1, tiled=True)  37 us
    pmax x1, blocking collectives, shards(): top_score = lax.pmax(local_top, ('kv', 'tp'))  37 us
    psum x2, blocking collectives, supply_the_scenes(): array_here = lax.psum(array_here, at)  25.6 us
    psum x1, blocking collectives, shards(): lax.psum((query_part, latent_part, rotary_part, square_part), 'tp')  13.4 us
  transfers between devices with their start and end apart: 3, of which 2 were waited for; matrix products, arithmetic and copies ran while one was open for 2% of the time, Pallas kernels for 0%

profile of v1, /device:TPU:0, one launch (start us, length us, event | category | flops | bytes accessed | tf_op | source)
XLA Modules:
  0.0 362.9 jit_solution(10456254263090970089)
XLA Ops:
  7.2 1.0 fusion.15
  8.2 1.5 fusion.20
  9.7 1.0 fusion.22
  10.7 1.1 fusion.24
  11.9 13.4 %all-reduce = (f32[16,4,96]{2,0,1:T(8,128)S(1)}, f32[16]{0:T(128)S(1)}, f32[16,128]{1,0:T(8,128)S(1)}, f32[16,32]{1,0:T(8,128)S(1)}) all-reduce(f32[16,4,96]{2,0,1:T(8,128)S(1)} %fusion.20, f32[16]{0:T(128)S(1)} %fusion.15, f32[16,128]{1,0:T(8,128)S(1)} %fusion.24, f32[16,32]{1,0:T(8,128)S(1)} %fusion.22), channel_id=1, replica_groups=mesh['kv'=8,'tp'=4] {'tp'}, use_global_device_ids=true, to_apply=%region_0.0 | all-reduce | flops 8720 | bytes 69760 | tf_op jit(solution)/shard_map/psum | solution.py:79
  25.3 0.1 multiply_convert_fusion.1
  25.3 1.7 fusion.1
  27.0 0.0 all-reduce.4.cloned.1.call-start
  27.1 0.7 convert_element_type.81
  27.8 0.1 broadcast_multiply_fusion
  27.8 0.1 subtract_convert_fusion.3
  28.0 0.1 slice_convert_fusion
  28.0 0.1 subtract_convert_fusion.2
  28.1 0.1 dynamic-slice_maximum_fusion
  28.2 0.1 copy.48
  28.3 41.5 %all-gather.1 = bf16[16,128,8]{0,2,1:T(8,128)(2,1)S(1)} all-gather(bf16[16,4,8]{0,2,1:T(8,128)(2,1)S(1)} %copy.48), channel_id=3, replica_groups=mesh['kv'=8,'tp'=4] {'kv','tp'}, dimensions={1}, use_global_device_ids=true | all-gather | bytes 33792 | tf_op jit(solution)/shard_map/all_gather | solution.py:98
  69.8 0.3 copy.50
  70.1 37.0 %all-gather.3 = bf16[32,32,16]{1,2,0:T(8,128)(2,1)S(1)} all-gather(bf16[1,32,16]{1,2,0:T(8,128)(2,1)S(1)} %get-tuple-element.20), channel_id=4, replica_groups=mesh['kv'=8,'tp'=4] {'kv','tp'}, dimensions={0}, use_global_device_ids=true | all-gather | bytes 33792 | tf_op jit(solution)/shard_map/all_gather | solution.py:99
  107.1 0.1 reshape.167
  107.3 0.1 fusion.54
  107.3 0.1 multiply_reduce_fusion
  107.5 0.7 broadcast_compare_fusion
  108.2 0.2 fusion.33
  108.4 0.1 bitcast_convert_fusion
  108.5 2.0 copy.75
  110.6 0.8 reshape.151
  111.3 3.7 %fusion.41 = f32[16,32,128]{2,1,0:T(8,128)S(1)} fusion(bf16[16,32,1024]{2,1,0:T(8,128)(2,1)S(1)} %reshape.151, bf16[16,128,1024]{2,1,0:T(8,128)(2,1)} %param.21), kind=kOutput, calls=%fused_computation.71 | convolution fusion | flops 134217728 | bytes 5505024 | tf_op jit(solution)/shard_map/bhr,bpr->bhp/dot_general | solution.py:120
  115.0 0.4 fusion.16
  115.4 0.3 select_reduce_fusion
  115.7 37.0 %pmax.7 = f32[16,32]{1,0:T(8,128)S(1)} all-reduce(f32[16,32]{1,0:T(8,128)S(1)} %get-tuple-element.11), channel_id=1, replica_groups=mesh['kv'=8,'tp'=4] {'kv','tp'}, use_global_device_ids=true, to_apply=%region_7.8 | all-reduce | flops 512 | bytes 4096 | tf_op jit(solution)/shard_map/pmax | solution.py:125
  152.7 2.9 fusion.9
  155.6 2.5 copy.52
  158.2 0.0 all-reduce.6.cloned.1.call-start
  158.2 103.9 %all-reduce.4.cloned.1.call-done = f32[16,32,1024]{2,0,1:T(8,128)} async-done(((f32[16,32,1024]{2,0,1:T(8,128)}), f32[16,32,1024]{2,0,1:T(8,128)}) %all-reduce.4.cloned.1.call-update) | async-done | bytes 2097168 | tf_op jit(solution)/shard_map/psum | solution.py:13
  262.1 0.7 pad_maximum_fusion
  262.8 0.7 dynamic-slice_bitcast_fusion
  263.5 2.1 constant_dynamic-slice_fusion
  265.6 0.3 fusion.7
  265.9 19.9 %psum.69 = f32[16,32]{1,0:T(8,128)S(1)} all-reduce(f32[16,32]{1,0:T(8,128)S(1)} %fusion.7), channel_id=1, replica_groups=mesh['kv'=8,'tp'=4] {'kv'}, use_global_device_ids=true, to_apply=%region_11.12 | all-reduce | flops 512 | bytes 4096 | tf_op jit(solution)/shard_map/psum | solution.py:13
  285.8 5.8 %psum.70 = f32[16,32]{1,0:T(8,128)S(1)} all-reduce(f32[16,32]{1,0:T(8,128)S(1)} %psum.69), channel_id=1, replica_groups=mesh['kv'=8,'tp'=4] {'tp'}, use_global_device_ids=true, to_apply=%region_12.13 | all-reduce | flops 512 | bytes 4096 | tf_op jit(solution)/shard_map/psum | solution.py:13
  291.5 0.1 dynamic-slice_add_fusion
  291.6 0.1 copy.53
  291.7 0.1 copy.54
  291.8 23.7 %all-reduce.6.cloned.1.call-done = f32[16,32,1024]{2,0,1:T(8,128)} async-done(((f32[16,32,1024]{2,0,1:T(8,128)}), f32[16,32,1024]{2,0,1:T(8,128)}) %all-reduce.6.cloned.1.call-update) | async-done | bytes 2097168 | tf_op jit(solution)/shard_map/psum | solution.py:13
  315.4 1.3 fusion.4
  316.7 1.3 fusion.3
  318.0 0.3 fusion.27
  318.2 38.1 %psum.71 = bf16[16,1024]{1,0:T(8,128)(2,1)} all-reduce(f32[16,1024]{1,0:T(8,128)S(1)} %fusion.27), channel_id=1, replica_groups=mesh['kv'=8,'tp'=4] {'kv'}, use_global_device_ids=true, to_apply=%region_13.14 | all-reduce | flops 16384 | bytes 98304 | tf_op jit(solution)/shard_map/psum | solution.py:145
  (18 shorter events, 0.2 us)
Async XLA Ops:
  7.2 310.8 %copy-start = (bf16[512,1024]{1,0:T(8,128)(2,1)S(1)}, bf16[512,1024]{1,0:T(8,128)(2,1)}, u32[]{:S(2)}) copy-start(bf16[512,1024]{1,0:T(8,128)(2,1)} %param.20) | copy-start | bytes 3145732
  7.2 101.2 %copy-start.2 = (f32[1024]{0:T(1024)S(1)}, f32[1024]{0:T(1024)}, u32[]{:S(2)}) copy-start(f32[1024]{0:T(1024)} %param.17) | copy-start | bytes 12292
  7.2 101.3 %all-gather.6.cloned.1.call-start = ((), (), s32[]{:S(2)}) async-start(), calls=%async_computation.2 | async-start | bytes 1081344 | tf_op jit(solution)/shard_map/all_gather | solution.py:97
  27.0 235.1 %all-reduce.4.cloned.1.call-start = ((), (), s32[]{:S(2)}) async-start(), calls=%async_computation | async-start | bytes 4194304 | tf_op jit(solution)/shard_map/psum | solution.py:13
  110.5 4.9 %copy-start.1 = (bf16[16,128,32]{1,2,0:T(8,128)(2,1)S(1)}, bf16[16,128,32]{1,2,0:T(8,128)(2,1)}, u32[]{:S(2)}) copy-start(bf16[16,128,32]{1,2,0:T(8,128)(2,1)} %param.22) | copy-start | bytes 393220
  158.2 157.3 %all-reduce.6.cloned.1.call-start = ((), (), s32[]{:S(2)}) async-start(), calls=%async_computation.1 | async-start | bytes 4194304 | tf_op jit(solution)/shard_map/psum | solution.py:13
Sparse Core Ops, SparseCore 0:
  27.1 54.0 all-gather.5
  158.3 103.7 all-reduce.3
  264.5 50.9 all-reduce.5
